TPU v7x, 128 devices: a whole 4x4x4 slice. The times are simulated.
128 devices in a mesh: ep: 16 (over z, x), tp: 8 (over y, core).
Axes of the slice: x: 4, y: 4, z: 4, core: 2. Of those that a mesh axis runs over, the one named last changes fastest.
Arguments:
- residual: bfloat16 [2048, 2048], P('ep', 'tp'), may hold values from -61 to 61
- in_gain: float32 [2048], replicated, may hold values from 0.1 to 1.9
- in_weight: bfloat16 [2048, 1024], P(None, 'tp'), may hold values from -0.125 to 0.125
- state: float32 [2, 2048, 4096], P(None, 'ep', 'tp'), may hold values from -3 to 3
- decay_rate: float32 [64, 64], P('tp'), may hold values from 0.1 to 1
- frequency: float32 [64, 64], P('tp'), may hold values from 0 to 200
- log_step: float32 [64], P('tp'), may hold values from -3 to -0.7
- in_coef: float32 [2, 64, 64, 16], P(None, 'tp'), may hold values from -1 to 1
- out_coef: float32 [2, 64, 16, 64], P(None, 'tp'), may hold values from -0.75 to 0.75
- skip_gain: float32 [1024], P('tp'), may hold values from -3 to 3
- out_weight: bfloat16 [1024, 2048], replicated, may hold values from -0.1875 to 0.1875
- mid_gain: float32 [2048], replicated, may hold values from 0.1 to 1.9
- gate_vector: bfloat16 [2048], replicated, may hold values from -0.125 to 0.125
- routes: int32 [2048, 4], P('ep'), may hold values from 0 to 127, all different within a row; in each aligned block of 128 rows (0 to 127, 128 to 255, ...) at most 8 rows name the same one
- route_weight: float32 [2048, 4], P('ep'), may hold values from 0.1 to 1
- expert_gate: bfloat16 [128, 2048, 512], P(('ep', 'tp')), may hold values from -0.125 to 0.125
- expert_up: bfloat16 [128, 2048, 512], P(('ep', 'tp')), may hold values from -0.125 to 0.125
- expert_down: bfloat16 [128, 512, 2048], P(('ep', 'tp')), may hold values from -0.25 to 0.25
- shared_gate: bfloat16 [2048, 4096], P(None, 'ep'), may hold values from -0.125 to 0.125
- shared_up: bfloat16 [2048, 4096], P(None, 'ep'), may hold values from -0.125 to 0.125
- shared_down: bfloat16 [4096, 2048], P('ep'), may hold values from -0.09375 to 0.09375
Outputs:
- layer_out: bfloat16 [2048, 2048], P(('ep', 'tp'))
- new_state: float32 [2, 2048, 4096], P(None, 'ep', 'tp')
Inputs may be any that keep to these rules, and one draw needn't show every extreme that they name: `routes`: each row names 4 different experts. Among the rows of one index of ep no expert is named more than 8 times, a bound that some block reaches.
All inputs are finite; a program needn't handle non-finite values.
Results may differ from a plain program's by a relative error of at most 0.0085.
Values may be sent and summed in bfloat16 or wider, within the bound.
No kernel may reach another device: no remote copies, remote signals or barrier semaphores. Data moves between devices by JAX's collectives and lax.ppermute only.
A program may use at most 128 MiB of HBM per device.

v0:
```python
import jax
import jax.numpy as jnp
from jax import lax
from jax.sharding import PartitionSpec as P

norm_eps = 1e-05
routed_scale = 2.5


def laid_out(blocks, dim):
    dims = list(blocks.shape[1:])
    dims[dim] *= blocks.shape[0]
    return jnp.moveaxis(blocks, 0, dim).reshape(dims)


def from_everyone(array, axis):
    length = lax.axis_size(axis)
    return lax.all_to_all(
        jnp.broadcast_to(array[None], (length, *array.shape)), axis, 0, 0, tiled=True
    )


def gather_directly(array, axis, dim):
    return laid_out(from_everyone(array, axis), dim)


def in_one_piece(arrays, axis, split_dim, concat_dim, along):
    both = jnp.concatenate(arrays, axis=along)
    result, at, finished = (
        lax.all_to_all(both, axis, split_axis=split_dim, concat_axis=concat_dim, tiled=True),
        0,
        [],
    )
    for a in arrays:
        finished.append(lax.slice_in_dim(result, at, at + a.shape[along], axis=along))
        at += a.shape[along]
    return tuple(finished)


def in_blocks(array, dim, length):
    before, after = (array.shape[:dim], array.shape[dim + 1 :])
    return jnp.moveaxis(array.reshape(*before, length, -1, *after), dim, 0)


def sent_and_summed(array, axis, dim):
    length = lax.axis_size(axis)
    blocks = lax.all_to_all(in_blocks(array, dim, length), axis, 0, 0, tiled=True)
    return jnp.sum(blocks.astype(jnp.float32), axis=0)


def layer_norm(values, gain_vec):
    row_mean = jnp.mean(values, axis=-1, keepdims=True)
    row_square = jnp.mean(values * values, axis=-1, keepdims=True)
    return (values - row_mean) * lax.rsqrt(row_square - row_mean * row_mean + norm_eps) * gain_vec


def coefficients(decay_rate, frequency, log_step, in_coef):
    time_step = jnp.exp(log_step)[:, None]
    real_rate = -decay_rate
    magnitude = jnp.exp(real_rate * time_step)
    keep_re = magnitude * jnp.cos(frequency * time_step)
    keep_im = magnitude * jnp.sin(frequency * time_step)
    denominator = real_rate * real_rate + frequency * frequency
    factor_re = ((keep_re - 1.0) * real_rate + keep_im * frequency) / denominator
    factor_im = (keep_im * real_rate - (keep_re - 1.0) * frequency) / denominator
    push_re = factor_re[..., None] * in_coef[0] - factor_im[..., None] * in_coef[1]
    push_im = factor_re[..., None] * in_coef[1] + factor_im[..., None] * in_coef[0]
    return (keep_re, keep_im, push_re, push_im)


def mixer_step(
    normed, in_weight, state, decay_rate, frequency, log_step, in_coef, out_coef, skip_gain
):
    row_count = normed.shape[0]
    group_count, state_count = decay_rate.shape
    keep_re, keep_im, push_re, push_im = coefficients(decay_rate, frequency, log_step, in_coef)
    drive = jnp.dot(normed, in_weight, preferred_element_type=jnp.float32).astype(jnp.bfloat16)
    drive_f = drive.astype(jnp.float32).reshape(row_count, group_count, -1)
    input_re = jnp.einsum("tgh,gph->tgp", drive_f, push_re)
    input_im = jnp.einsum("tgh,gph->tgp", drive_f, push_im)
    old_re = state[0].reshape(row_count, group_count, state_count)
    old_im = state[1].reshape(row_count, group_count, state_count)
    new_re = keep_re * old_re - keep_im * old_im + input_re
    new_im = keep_re * old_im + keep_im * old_re + input_im
    read_out = jnp.einsum("ghp,tgp->tgh", out_coef[0], new_re) - jnp.einsum(
        "ghp,tgp->tgh", out_coef[1], new_im
    )
    read_out = read_out.reshape(row_count, -1) + skip_gain * drive_f.reshape(row_count, -1)
    mixed_rows = jax.nn.gelu(read_out, approximate=True).astype(jnp.bfloat16)
    updated = jnp.stack([new_re.reshape(row_count, -1), new_im.reshape(row_count, -1)])
    return (mixed_rows, updated)


def route_slots(routes, experts):
    flat_routes = routes.reshape(-1)
    onehot = (flat_routes[:, None] == jnp.arange(experts, dtype=jnp.int32)[None, :]).astype(
        jnp.int32
    )
    before = jnp.cumsum(onehot, axis=0) - onehot
    return jnp.sum(before * onehot, axis=1).reshape(routes.shape)


def expert_block(row_block, gate_weight, up_weight, down_weight):
    gate_part = jnp.dot(row_block, gate_weight, preferred_element_type=jnp.float32)
    up_part = jnp.dot(row_block, up_weight, preferred_element_type=jnp.float32)
    hidden = (jax.nn.silu(gate_part) * up_part).astype(jnp.bfloat16)
    return jnp.dot(hidden, down_weight, preferred_element_type=jnp.float32).astype(jnp.bfloat16)


def per_device(
    residual,
    in_gain,
    in_weight,
    state,
    decay_rate,
    frequency,
    log_step,
    in_coef,
    out_coef,
    skip_gain,
    out_weight,
    mid_gain,
    gate_vector,
    routes,
    route_weight,
    expert_gate,
    expert_up,
    expert_down,
    shared_gate,
    shared_up,
    shared_down,
):
    tp_count = lax.axis_size("tp")
    ep_count = lax.axis_size("ep")
    tp_place = lax.axis_index("tp")
    seq_rows, feat_part = residual.shape
    width = feat_part * tp_count
    full_resid = gather_directly(residual, "tp", 1)
    normed = layer_norm(full_resid.astype(jnp.float32), in_gain).astype(jnp.bfloat16)
    mixed_part, new_state = mixer_step(
        normed, in_weight, state, decay_rate, frequency, log_step, in_coef, out_coef, skip_gain
    )
    mixed_rows = lax.all_gather(mixed_part, "tp", axis=1, tiled=True)
    after_mix = full_resid.astype(jnp.float32) + jnp.dot(
        mixed_rows, out_weight, preferred_element_type=jnp.float32
    )
    normed_mid = layer_norm(after_mix, mid_gain).astype(jnp.bfloat16)
    per_dev = seq_rows // tp_count
    own_mid = lax.dynamic_slice_in_dim(normed_mid, tp_place * per_dev, per_dev, 0)
    own_after = lax.dynamic_slice_in_dim(after_mix, tp_place * per_dev, per_dev, 0)
    experts = ep_count * tp_count
    top_count = routes.shape[1]
    capacity = max(2, 2 * seq_rows * top_count // experts)
    slot_rank = route_slots(routes, experts)
    dest_tp = routes % tp_count
    dest_ep = routes // tp_count
    is_mine = dest_tp == tp_place
    slot_place = dest_ep * capacity + slot_rank
    slot_total = ep_count * capacity
    matches = (
        slot_place.reshape(-1)[None, :] == jnp.arange(slot_total, dtype=jnp.int32)[:, None]
    ) & is_mine.reshape(-1)[None, :]
    token_ids = jnp.repeat(jnp.arange(seq_rows, dtype=jnp.int32), top_count)
    slot_token = jnp.sum(jnp.where(matches, token_ids[None, :], 0), axis=1)
    outgoing = normed_mid[slot_token].reshape(ep_count, capacity, width)
    copies = jnp.broadcast_to(own_mid[None], (ep_count, per_dev, width))
    got_slots, got_rows = in_one_piece((outgoing, copies), "ep", 0, 0, 1)
    flat_rows = got_slots.reshape(-1, width)
    result = expert_block(flat_rows, expert_gate[0], expert_up[0], expert_down[0])
    computed = result.reshape(got_slots.shape)
    returned = lax.all_to_all(computed, "ep", split_axis=0, concat_axis=0, tiled=True)
    piece = got_rows.reshape(-1, width)
    gate_part = jnp.dot(piece, shared_gate, preferred_element_type=jnp.float32)
    up_part = jnp.dot(piece, shared_up, preferred_element_type=jnp.float32)
    shared_hidden = (jax.nn.silu(gate_part) * up_part).astype(jnp.bfloat16)
    partial_rows = jnp.dot(shared_hidden, shared_down, preferred_element_type=jnp.float32)
    partial_back = lax.all_to_all(
        partial_rows.reshape(ep_count, per_dev, width).astype(jnp.bfloat16),
        "ep",
        split_axis=0,
        concat_axis=0,
        tiled=True,
    ).astype(jnp.float32)
    shared = jnp.sum(partial_back, axis=0)
    flat_back = returned.reshape(slot_total, width)
    weights = route_weight / jnp.sum(route_weight, axis=-1, keepdims=True) * routed_scale
    picked = flat_back[jnp.where(is_mine, slot_place, 0)].astype(jnp.float32)
    routed_part = jnp.sum(jnp.where(is_mine, weights, 0.0)[..., None] * picked, axis=1)
    routed = sent_and_summed(routed_part.astype(jnp.bfloat16), "tp", 0)
    gate_value = jax.nn.sigmoid(jnp.dot(own_mid, gate_vector, preferred_element_type=jnp.float32))
    layer_out = (own_after + routed + gate_value[:, None] * shared).astype(jnp.bfloat16)
    return (layer_out, new_state)


def solution(mesh):
    return jax.shard_map(
        per_device,
        mesh=mesh,
        in_specs=(
            P("ep", "tp"),
            P(),
            P(None, "tp"),
            P(None, "ep", "tp"),
            P("tp", None),
            P("tp", None),
            P("tp"),
            P(None, "tp", None, None),
            P(None, "tp", None, None),
            P("tp"),
            P(),
            P(),
            P(),
            P("ep", None),
            P("ep", None),
            P(("ep", "tp"), None, None),
            P(("ep", "tp"), None, None),
            P(("ep", "tp"), None, None),
            P(None, "ep"),
            P(None, "ep"),
            P("ep", None),
        ),
        out_specs=(P(("ep", "tp"), None), P(None, "ep", "tp")),
        check_vma=False,
    )
```

profile of v0, /device:TPU:0, one launch (start us, length us, event | category | flops | bytes accessed | tf_op | source)
XLA Modules:
  0.0 138.5 jit_solution(16512454888797237247)
XLA Ops:
  0.7 1.8 %broadcast_in_dim.22 = bf16[8,128,256]{2,1,0:T(8,128)(2,1)} broadcast(bf16[128,256]{1,0:T(8,128)(2,1)} %param.21), dimensions={1,2} | broadcast | bytes 589824 | tf_op jit(solution)/shard_map/broadcast_in_dim | solution.py:19
  2.5 4.6 %all-to-all-start = ((bf16[8,128,256]{2,1,0:T(8,128)(2,1)}), bf16[8,128,256]{2,1,0:T(8,128)(2,1)S(1)}, u32[]{:S(2)}, u32[]{:S(2)}) async-start(bf16[8,128,256]{2,1,0:T(8,128)(2,1)} %broadcast_in_dim.22), calls=%async_computation | async-start | bytes 1048576 | tf_op jit(solution)/shard_map/all_to_all | solution.py:18
  7.1 0.8 copy.88
  7.8 0.1 eq.54
  8.0 0.1 eq.50
  8.1 0.7 exp.17
  8.7 0.7 reduce_sum.94
  9.4 0.7 multiply_select_fusion
  10.1 0.1 copy.94
  10.3 0.1 and.23
  10.4 0.1 copy.90
  10.6 0.1 broadcast_in_dim.25
  10.7 0.2 fusion.37
  11.0 0.2 fusion.26
  11.2 0.1 reshape.121
  11.4 0.1 copy.93
  11.5 0.1 eq.58
  11.6 1.1 fusion.78
  12.7 0.1 copy.85
  12.8 0.1 copy.86
  13.0 0.1 select_reduce_fusion
  13.2 0.1 add_divide_fusion
  13.3 4.1 %all-to-all-done = bf16[8,128,256]{2,1,0:T(8,128)(2,1)S(1)} async-done(((bf16[8,128,256]{2,1,0:T(8,128)(2,1)}), bf16[8,128,256]{2,1,0:T(8,128)(2,1)S(1)}, u32[]{:S(2)}, u32[]{:S(2)}) %all-to-all-start) | async-done | bytes 524320 | tf_op jit(solution)/shard_map/all_to_all | solution.py:18
  17.6 0.2 convert_reduce_fusion.1
  17.8 0.6 copy-done.7
  18.4 0.4 convolution_convert_fusion.2
  18.9 0.3 fusion.9
  19.2 0.3 fusion.10
  19.5 0.1 fusion.52
  19.6 0.1 convolution_subtract_fusion
  19.8 0.1 fusion.50
  19.9 12.8 %all_gather.3 = bf16[128,1024]{0,1:T(8,128)(2,1)S(1)} all-gather(bf16[128,128]{0,1:T(8,128)(2,1)S(1)} %fusion.50), channel_id=1, replica_groups=mesh['ep'=16,'tp'=8] {'tp'}, dimensions={1}, use_global_device_ids=true | all-gather | bytes 294912 | tf_op jit(solution)/shard_map/all_gather | solution.py:143
  32.7 0.8 fusion.75
  33.6 1.0 copy-done.2
  34.6 0.2 multiply_convert_fusion
  34.8 0.9 gather_fusion
  35.8 0.1 broadcast_in_dim.32
  35.9 0.2 pad_maximum_fusion
  36.1 31.1 %all_to_all.25 = bf16[16,24,2048]{2,1,0:T(8,128)(2,1)S(1)} all-to-all(bf16[16,24,2048]{2,1,0:T(8,128)(2,1)S(1)} %pad_maximum_fusion), channel_id=1, replica_groups=mesh['ep'=16,'tp'=8] {'ep'}, dimensions={0} | all-to-all | bytes 3145728 | tf_op jit(solution)/shard_map/all_to_all | solution.py:30
  67.1 1.2 copy-done.1
  68.3 0.4 fusion.4
  68.8 3.4 %fusion = bf16[16,8,2048]{2,1,0:T(8,128)(2,1)} fusion(bf16[1,512,2048]{2,1,0:T(8,128)(2,1)S(1)} %copy-done, bf16[1,2048,512]{2,1,0:T(8,128)(2,1)} %param.37, bf16[16,24,2048]{2,1,0:T(8,128)(2,1)} %copy-done.1, f32[128,512]{1,0:T(8,128)S(1)} %fusion.4), kind=kOutput, calls=%fused_computation.6 | convolution fusion | flops 537526272 | bytes 5505024 | tf_op jit(solution)/shard_map/dot_general | solution.py:107
  72.2 3.6 %all-to-all-start.2 = ((bf16[16,8,2048]{2,1,0:T(8,128)(2,1)}), bf16[16,8,2048]{2,1,0:T(8,128)(2,1)S(1)}, u32[]{:S(2)}, u32[]{:S(2)}) async-start(bf16[16,8,2048]{2,1,0:T(8,128)(2,1)} %fusion), calls=%async_computation.2 | async-start | bytes 1048576 | tf_op jit(solution)/shard_map/all_to_all | solution.py:171
  75.7 0.1 copy.87
  75.9 0.1 copy.95
  76.0 0.1 reshape.138
  76.1 2.3 %slice.48 = bf16[16,16,2048]{2,1,0:T(8,128)(2,1)} slice(bf16[16,24,2048]{2,1,0:T(8,128)(2,1)} %copy-done.1), slice={[0:16], [8:24], [0:2048]} | slice | bytes 2097152 | tf_op jit(solution)/shard_map/slice | solution.py:35
  78.4 8.2 %all-to-all-done.2 = bf16[16,8,2048]{2,1,0:T(8,128)(2,1)S(1)} async-done(((bf16[16,8,2048]{2,1,0:T(8,128)(2,1)}), bf16[16,8,2048]{2,1,0:T(8,128)(2,1)S(1)}, u32[]{:S(2)}, u32[]{:S(2)}) %all-to-all-start.2) | async-done | bytes 524320 | tf_op jit(solution)/shard_map/all_to_all | solution.py:171
  86.6 3.3 %gather_fusion.1 = bf16[512,2048]{1,0:T(8,128)(2,1)} fusion(bf16[128,2048]{1,0:T(8,128)(2,1)S(1)} %bitcast.115, s32[1024]{0:T(1024)S(1)} %pad_clamp_fusion), kind=kCustom, calls=%fused_computation.1 | custom fusion | bytes 4196352 | tf_op jit(solution)/shard_map/gather | solution.py:187
  89.9 4.8 %reshape.146 = f32[128,4,2048]{2,1,0:T(4,128)} reshape(bf16[512,2048]{1,0:T(8,128)(2,1)} %gather_fusion.1) | data formatting | bytes 6291456 | tf_op jit(solution)/shard_map/convert_element_type | solution.py:187
  94.7 6.3 %multiply_reduce_fusion = bf16[128,2048]{1,0:T(8,128)(2,1)} fusion(f32[128,4,2048]{2,1,0:T(4,128)} %reshape.146, f32[128,4]{1,0:T(8,128)S(1)} %copy.87), kind=kLoop, calls=%fused_computation.2 | loop fusion | flops 1835008 | bytes 4720640 | tf_op jit(solution)/shard_map/reduce_sum | solution.py:188
  100.9 4.1 %all-to-all-start.3 = ((bf16[8,16,2048]{2,1,0:T(8,128)(2,1)}), bf16[8,16,2048]{2,1,0:T(8,128)(2,1)}, u32[]{:S(2)}, u32[]{:S(2)}) async-start(bf16[8,16,2048]{2,1,0:T(8,128)(2,1)} %bitcast.126), calls=%async_computation.3 | async-start | bytes 1048576 | tf_op jit(solution)/shard_map/all_to_all | solution.py:47
  105.1 2.4 %fusion.79 = f32[256,256]{1,0:T(8,128)} fusion(bf16[256,2048]{1,0:T(8,128)(2,1)S(1)} %bitcast.118, bf16[2048,256]{1,0:T(8,128)(2,1)} %param.39), kind=kOutput, calls=%fused_computation.129 | convolution fusion | flops 268435456 | bytes 2359296 | tf_op jit(solution)/shard_map/dot_general | solution.py:173
  107.5 3.9 %convolution_convert_fusion = bf16[256,2048]{1,0:T(8,128)(2,1)} fusion(bf16[256,2048]{1,0:T(8,128)(2,1)} %param.41, bf16[256,2048]{1,0:T(8,128)(2,1)S(1)} %bitcast.119, bf16[2048,256]{1,0:T(8,128)(2,1)} %param.40, f32[256,256]{1,0:T(8,128)} %fusion.79), kind=kOutput, calls=%fused_computation.3 | convolution fusion | flops 537788416 | bytes 4456448 | tf_op jit(solution)/shard_map/dot_general | solution.py:176
  111.4 4.0 %all-to-all-done.3 = bf16[8,16,2048]{2,1,0:T(8,128)(2,1)} async-done(((bf16[8,16,2048]{2,1,0:T(8,128)(2,1)}), bf16[8,16,2048]{2,1,0:T(8,128)(2,1)}, u32[]{:S(2)}, u32[]{:S(2)}) %all-to-all-start.3) | async-done | bytes 524320 | tf_op jit(solution)/shard_map/all_to_all | solution.py:47
  115.4 3.7 %all-to-all-start.4 = ((bf16[16,16,2048]{2,1,0:T(8,128)(2,1)}), bf16[16,16,2048]{2,1,0:T(8,128)(2,1)S(1)}, u32[]{:S(2)}, u32[]{:S(2)}) async-start(bf16[16,16,2048]{2,1,0:T(8,128)(2,1)} %bitcast.129), calls=%async_computation.4 | async-start | bytes 2097152 | tf_op jit(solution)/shard_map/all_to_all | solution.py:177
  119.1 1.8 %copy.97 = f32[1,128,512]{2,1,0:T(8,128)} copy(f32[1,128,512]{1,2,0:T(8,128)} %bitcast.125) | data formatting | bytes 524288 | tf_op jit(solution)/shard_map/stack;reshape | solution.py:90
  120.9 0.8 copy.96
  121.7 1.9 %pad_maximum_fusion.1 = f32[2,128,512]{2,1,0:T(8,128)} fusion(f32[1,128,512]{2,1,0:T(8,128)} %copy.97, f32[1,128,512]{2,1,0:T(8,128)} %copy.96), kind=kLoop, calls=%fused_computation.38 | loop fusion | flops 131072 | bytes 1048576 | tf_op jit(solution)/shard_map/stack | solution.py:90
  123.6 0.1 fusion.18
  123.7 1.1 convert_reduce_fusion.2
  124.9 11.8 %all-to-all-done.4 = bf16[16,16,2048]{2,1,0:T(8,128)(2,1)S(1)} async-done(((bf16[16,16,2048]{2,1,0:T(8,128)(2,1)}), bf16[16,16,2048]{2,1,0:T(8,128)(2,1)S(1)}, u32[]{:S(2)}, u32[]{:S(2)}) %all-to-all-start.4) | async-done | bytes 1048608 | tf_op jit(solution)/shard_map/all_to_all | solution.py:177
  136.7 0.1 convert_reduce_fusion
  136.8 1.6 %add_convert_fusion = bf16[16,2048]{1,0:T(8,128)(2,1)} fusion(f32[16,2048]{1,0:T(8,128)S(1)} %convert_reduce_fusion, f32[16,2048]{1,0:T(8,128)S(1)} %convert_reduce_fusion.2, f32[128,2048]{1,0:T(8,128)} %copy-done.2, s32[]{:T(128)S(6)} %select_n.41, f32[16]{0:T(128)S(1)} %fusion.18), kind=kLoop, calls=%fused_computation.62 | loop fusion | flops 131072 | bytes 458820 | tf_op jit(solution)/shard_map/convert_element_type | solution.py:191
  (49 shorter events, 0.5 us)
Async XLA Ops:
  0.6 68.1 %copy-start = (bf16[1,512,2048]{2,1,0:T(8,128)(2,1)S(1)}, bf16[1,512,2048]{2,1,0:T(8,128)(2,1)}, u32[]{:S(2)}) copy-start(bf16[1,512,2048]{2,1,0:T(8,128)(2,1)} %param.38) | copy-start | bytes 6291460
  0.6 10.7 %copy-start.10 = (s32[128,4]{0,1:T(4,128)S(1)}, s32[128,4]{0,1:T(4,128)}, u32[]{:S(2)}) copy-start(s32[128,4]{0,1:T(4,128)} %param.34) | copy-start | bytes 6148
  2.5 14.9 %all-to-all-start = ((bf16[8,128,256]{2,1,0:T(8,128)(2,1)}), bf16[8,128,256]{2,1,0:T(8,128)(2,1)S(1)}, u32[]{:S(2)}, u32[]{:S(2)}) async-start(bf16[8,128,256]{2,1,0:T(8,128)(2,1)} %broadcast_in_dim.22), calls=%async_computation | async-start | bytes 1048576 | tf_op jit(solution)/shard_map/all_to_all | solution.py:18
  10.5 2.6 %copy-start.13 = (f32[8,64]{1,0:T(8,128)S(1)}, f32[8,64]{1,0:T(8,128)}, u32[]{:S(2)}) copy-start(f32[8,64]{1,0:T(8,128)} %param.26) | copy-start | bytes 6148
  10.5 2.6 %copy-start.14 = (f32[8,64]{1,0:T(8,128)S(1)}, f32[8,64]{1,0:T(8,128)}, u32[]{:S(2)}) copy-start(f32[8,64]{1,0:T(8,128)} %param.25) | copy-start | bytes 6148
  13.3 4.6 %copy-start.11 = (f32[2048]{0:T(1024)S(1)}, f32[2048]{0:T(1024)}, u32[]{:S(2)}) copy-start(f32[2048]{0:T(1024)} %param.22) | copy-start | bytes 24580
  17.4 1.0 copy-start.7
  17.5 1.4 copy-start.8
  17.6 1.9 %copy-start.9 = (f32[2,8,16,64]{3,2,1,0:T(8,128)S(1)}, f32[2,8,16,64]{3,2,1,0:T(8,128)}, u32[]{:S(2)}) copy-start(f32[2,8,16,64]{3,2,1,0:T(8,128)} %param.29) | copy-start | bytes 196612
  18.4 1.4 copy-start.16
  18.4 14.3 %copy-start.3 = (bf16[1024,2048]{1,0:T(8,128)(2,1)S(1)}, bf16[1024,2048]{1,0:T(8,128)(2,1)}, u32[]{:S(2)}) copy-start(bf16[1024,2048]{1,0:T(8,128)(2,1)} %param.31) | copy-start | bytes 12582916
  19.2 14.4 %copy-start.5 = (f32[128,8,64]{0,2,1:T(8,128)}, f32[128,8,64]{0,2,1:T(8,128)S(1)}, u32[]{:S(2)}) copy-start(f32[128,8,64]{0,2,1:T(8,128)S(1)} %fusion.9) | copy-start | bytes 786436
  32.7 1.9 %copy-start.12 = (f32[2048]{0:T(1024)S(1)}, f32[2048]{0:T(1024)}, u32[]{:S(2)}) copy-start(f32[2048]{0:T(1024)} %param.32) | copy-start | bytes 24580
  33.6 1.0 copy-start.2
  36.0 32.3 %copy-start.6 = (bf16[1,2048,512]{2,1,0:T(8,128)(2,1)S(1)}, bf16[1,2048,512]{2,1,0:T(8,128)(2,1)}, u32[]{:S(2)}) copy-start(bf16[1,2048,512]{2,1,0:T(8,128)(2,1)} %param.36) | copy-start | bytes 6291460
  67.1 1.2 copy-start.1
  72.2 14.4 %all-to-all-start.2 = ((bf16[16,8,2048]{2,1,0:T(8,128)(2,1)}), bf16[16,8,2048]{2,1,0:T(8,128)(2,1)S(1)}, u32[]{:S(2)}, u32[]{:S(2)}) async-start(bf16[16,8,2048]{2,1,0:T(8,128)(2,1)} %fusion), calls=%async_computation.2 | async-start | bytes 1048576 | tf_op jit(solution)/shard_map/all_to_all | solution.py:171
  94.7 10.4 %copy-start.4 = (bf16[16,16,2048]{2,1,0:T(8,128)(2,1)S(1)}, bf16[16,16,2048]{2,1,0:T(8,128)(2,1)}, u32[]{:S(2)}) copy-start(bf16[16,16,2048]{2,1,0:T(8,128)(2,1)} %slice.48) | copy-start | bytes 3145732
  100.9 14.5 %all-to-all-start.3 = ((bf16[8,16,2048]{2,1,0:T(8,128)(2,1)}), bf16[8,16,2048]{2,1,0:T(8,128)(2,1)}, u32[]{:S(2)}, u32[]{:S(2)}) async-start(bf16[8,16,2048]{2,1,0:T(8,128)(2,1)} %bitcast.126), calls=%async_computation.3 | async-start | bytes 1048576 | tf_op jit(solution)/shard_map/all_to_all | solution.py:47
  111.4 7.7 %copy-start.15 = (bf16[2048]{0:T(1024)(128)(2,1)S(1)}, bf16[2048]{0:T(1024)(128)(2,1)}, u32[]{:S(2)}) copy-start(bf16[2048]{0:T(1024)(128)(2,1)} %param.33) | copy-start | bytes 12292
  115.4 21.3 %all-to-all-start.4 = ((bf16[16,16,2048]{2,1,0:T(8,128)(2,1)}), bf16[16,16,2048]{2,1,0:T(8,128)(2,1)S(1)}, u32[]{:S(2)}, u32[]{:S(2)}) async-start(bf16[16,16,2048]{2,1,0:T(8,128)(2,1)} %bitcast.129), calls=%async_computation.4 | async-start | bytes 2097152 | tf_op jit(solution)/shard_map/all_to_all | solution.py:177
where the time goes:
time: 139 us; the launch traced here: 138 us
  blocking collectives  43.9 us (32%)
  waiting for transfers between devices  28.1 us (20%)
  local copies, waits for them, and re-layouts  23 us (17%)
  starting transfers between devices  16 us (12%)
  other arithmetic  14.1 us (10%)
  matrix products  12.4 us (9%)
    all_to_all x1, blocking collectives, in_one_piece(): lax.all_to_all(both, axis, split_axis=split_dim, concat_axis=concat_dim,...  31.1 us
    all_gather x1, blocking collectives, per_device(): mixed_rows = lax.all_gather(mixed_part, 'tp', axis=1, tiled=True)  12.8 us
    all_to_all x1, waiting for transfers between devices, per_device(): lax.all_to_all(partial_rows.reshape(ep_count, per_dev, width).astype(jnp....  11.8 us
    all_to_all x1, waiting for transfers between devices, per_device(): lax.all_to_all(computed, 'ep', split_axis=0, concat_axis=0, tiled=True)  8.19 us
    reduce_sum x1, other arithmetic, per_device(): jnp.sum(jnp.where(is_mine, weights, 0.0)[..., None] * picked, axis=1)  6.28 us
    convert_element_type x1, local copies, waits for them, and re-layouts, per_device(): picked = flat_back[jnp.where(is_mine, slot_place, 0)].astype(jnp.float32)  4.75 us
    all_to_all x1, starting transfers between devices, from_everyone(): lax.all_to_all(jnp.broadcast_to(array[None], (length, *array.shape)), axi...  4.58 us
    all_to_all x1, starting transfers between devices, sent_and_summed(): lax.all_to_all(in_blocks(array, dim, length), axis, 0, 0, tiled=True)  4.14 us
  transfers between devices with their start and end apart: 4, of which 4 were waited for; matrix products, arithmetic and copies ran while one was open for 15% of the time, Pallas kernels for 0%

commit v1 on v0

--- a/solution.py
+++ b/solution.py
@@ -140,7 +140,12 @@
     mixed_part, new_state = mixer_step(
         normed, in_weight, state, decay_rate, frequency, log_step, in_coef, out_coef, skip_gain
     )
-    mixed_rows = lax.all_gather(mixed_part, "tp", axis=1, tiled=True)
+
+    def stops_all_view(arr):
+        work_now = lax.all_gather(arr, axis_name="tp")
+        return jnp.concatenate(work_now, axis=1)
+
+    mixed_rows = stops_all_view(mixed_part)
     after_mix = full_resid.astype(jnp.float32) + jnp.dot(
         mixed_rows, out_weight, preferred_element_type=jnp.float32
     )

time: 139 us -> 138 us (level)
  no operation moved by 1% of the time
where the time goes in v1:
time: 138 us; the launch traced here: 137 us
  blocking collectives  42.6 us (31%)
  waiting for transfers between devices  28.2 us (20%)
  local copies, waits for them, and re-layouts  23 us (17%)
  starting transfers between devices  16 us (12%)
  other arithmetic  14.1 us (10%)
  matrix products  12.4 us (9%)
    all_to_all x1, blocking collectives, in_one_piece(): lax.all_to_all(both, axis, split_axis=split_dim, concat_axis=concat_dim,...  31.1 us
    all_to_all x1, waiting for transfers between devices, per_device(): lax.all_to_all(partial_rows.reshape(ep_count, per_dev, width).astype(jnp....  11.8 us
    all_gather x1, blocking collectives, stops_all_view(): work_now = lax.all_gather(arr, axis_name='tp')  11.5 us
    all_to_all x1, waiting for transfers between devices, per_device(): lax.all_to_all(computed, 'ep', split_axis=0, concat_axis=0, tiled=True)  8.2 us
    reduce_sum x1, other arithmetic, per_device(): jnp.sum(jnp.where(is_mine, weights, 0.0)[..., None] * picked, axis=1)  6.28 us
    convert_element_type x1, local copies, waits for them, and re-layouts, per_device(): picked = flat_back[jnp.where(is_mine, slot_place, 0)].astype(jnp.float32)  4.75 us
    all_to_all x1, starting transfers between devices, from_everyone(): lax.all_to_all(jnp.broadcast_to(array[None], (length, *array.shape)), axi...  4.58 us
    all_to_all x1, starting transfers between devices, sent_and_summed(): lax.all_to_all(in_blocks(array, dim, length), axis, 0, 0, tiled=True)  4.14 us
  transfers between devices with their start and end apart: 4, of which 4 were waited for; matrix products, arithmetic and copies ran while one was open for 15% of the time, Pallas kernels for 0%

profile of v1, /device:TPU:0, one launch (start us, length us, event | category | flops | bytes accessed | tf_op | source)
XLA Modules:
  0.0 137.2 jit_solution(3782610992156359546)
XLA Ops:
  0.7 1.8 %broadcast_in_dim.22 = bf16[8,128,256]{2,1,0:T(8,128)(2,1)} broadcast(bf16[128,256]{1,0:T(8,128)(2,1)} %param.21), dimensions={1,2} | broadcast | bytes 589824 | tf_op jit(solution)/shard_map/broadcast_in_dim | solution.py:19
  2.5 4.6 %all-to-all-start = ((bf16[8,128,256]{2,1,0:T(8,128)(2,1)}), bf16[8,128,256]{2,1,0:T(8,128)(2,1)S(1)}, u32[]{:S(2)}, u32[]{:S(2)}) async-start(bf16[8,128,256]{2,1,0:T(8,128)(2,1)} %broadcast_in_dim.22), calls=%async_computation | async-start | bytes 1048576 | tf_op jit(solution)/shard_map/all_to_all | solution.py:18
  7.1 0.8 copy.92
  7.8 0.1 eq.54
  8.0 0.1 eq.50
  8.1 0.7 exp.17
  8.7 0.7 reduce_sum.94
  9.4 0.7 multiply_select_fusion
  10.1 0.1 copy.98
  10.3 0.1 and.23
  10.4 0.1 copy.94
  10.6 0.1 broadcast_in_dim.25
  10.7 0.2 fusion.37
  11.0 0.2 fusion.26
  11.2 0.1 reshape.129
  11.4 0.1 copy.97
  11.5 0.1 eq.58
  11.6 1.1 fusion.78
  12.7 0.1 copy.88
  12.8 0.1 copy.89
  13.0 0.1 select_reduce_fusion
  13.2 0.1 add_divide_fusion
  13.3 4.1 %all-to-all-done = bf16[8,128,256]{2,1,0:T(8,128)(2,1)S(1)} async-done(((bf16[8,128,256]{2,1,0:T(8,128)(2,1)}), bf16[8,128,256]{2,1,0:T(8,128)(2,1)S(1)}, u32[]{:S(2)}, u32[]{:S(2)}) %all-to-all-start) | async-done | bytes 524320 | tf_op jit(solution)/shard_map/all_to_all | solution.py:18
  17.6 0.2 convert_reduce_fusion.1
  17.8 0.6 copy-done.7
  18.4 0.4 convolution_convert_fusion.2
  18.9 0.3 fusion.9
  19.2 0.3 fusion.10
  19.5 0.1 fusion.52
  19.6 0.1 convolution_subtract_fusion
  19.8 0.1 fusion.50
  19.9 11.5 %all-gather = bf16[1024,128]{0,1:T(8,128)(2,1)S(1)} all-gather(bf16[128,128]{0,1:T(8,128)(2,1)S(1)} %fusion.50), channel_id=2, replica_groups=mesh['ep'=16,'tp'=8] {'tp'}, dimensions={0}, use_global_device_ids=true | all-gather | bytes 294912 | tf_op jit(solution)/shard_map/all_gather | solution.py:145
  31.5 0.8 fusion.75
  32.4 1.0 copy-done.2
  33.3 0.2 multiply_convert_fusion
  33.6 0.9 gather_fusion
  34.5 0.1 broadcast_in_dim.32
  34.6 0.2 pad_maximum_fusion
  34.8 31.1 %all_to_all.25 = bf16[16,24,2048]{2,1,0:T(8,128)(2,1)S(1)} all-to-all(bf16[16,24,2048]{2,1,0:T(8,128)(2,1)S(1)} %pad_maximum_fusion), channel_id=1, replica_groups=mesh['ep'=16,'tp'=8] {'ep'}, dimensions={0} | all-to-all | bytes 3145728 | tf_op jit(solution)/shard_map/all_to_all | solution.py:30
  65.9 1.2 copy-done.1
  67.1 0.4 fusion.4
  67.5 3.4 %fusion = bf16[16,8,2048]{2,1,0:T(8,128)(2,1)} fusion(bf16[1,512,2048]{2,1,0:T(8,128)(2,1)S(1)} %copy-done, bf16[1,2048,512]{2,1,0:T(8,128)(2,1)} %param.37, bf16[16,24,2048]{2,1,0:T(8,128)(2,1)} %copy-done.1, f32[128,512]{1,0:T(8,128)S(1)} %fusion.4), kind=kOutput, calls=%fused_computation.6 | convolution fusion | flops 537526272 | bytes 5505024 | tf_op jit(solution)/shard_map/dot_general | solution.py:107
  70.9 3.6 %all-to-all-start.2 = ((bf16[16,8,2048]{2,1,0:T(8,128)(2,1)}), bf16[16,8,2048]{2,1,0:T(8,128)(2,1)S(1)}, u32[]{:S(2)}, u32[]{:S(2)}) async-start(bf16[16,8,2048]{2,1,0:T(8,128)(2,1)} %fusion), calls=%async_computation.2 | async-start | bytes 1048576 | tf_op jit(solution)/shard_map/all_to_all | solution.py:176
  74.5 0.1 copy.91
  74.6 0.1 copy.99
  74.7 0.1 reshape.146
  74.8 2.3 %slice.48 = bf16[16,16,2048]{2,1,0:T(8,128)(2,1)} slice(bf16[16,24,2048]{2,1,0:T(8,128)(2,1)} %copy-done.1), slice={[0:16], [8:24], [0:2048]} | slice | bytes 2097152 | tf_op jit(solution)/shard_map/slice | solution.py:35
  77.2 8.2 %all-to-all-done.2 = bf16[16,8,2048]{2,1,0:T(8,128)(2,1)S(1)} async-done(((bf16[16,8,2048]{2,1,0:T(8,128)(2,1)}), bf16[16,8,2048]{2,1,0:T(8,128)(2,1)S(1)}, u32[]{:S(2)}, u32[]{:S(2)}) %all-to-all-start.2) | async-done | bytes 524320 | tf_op jit(solution)/shard_map/all_to_all | solution.py:176
  85.4 3.3 %gather_fusion.1 = bf16[512,2048]{1,0:T(8,128)(2,1)} fusion(bf16[128,2048]{1,0:T(8,128)(2,1)S(1)} %bitcast.123, s32[1024]{0:T(1024)S(1)} %pad_clamp_fusion), kind=kCustom, calls=%fused_computation.1 | custom fusion | bytes 4196352 | tf_op jit(solution)/shard_map/gather | solution.py:192
  88.7 4.8 %reshape.155 = f32[128,4,2048]{2,1,0:T(4,128)} reshape(bf16[512,2048]{1,0:T(8,128)(2,1)} %gather_fusion.1) | data formatting | bytes 6291456 | tf_op jit(solution)/shard_map/convert_element_type | solution.py:192
  93.4 6.3 %multiply_reduce_fusion = bf16[128,2048]{1,0:T(8,128)(2,1)} fusion(f32[128,4,2048]{2,1,0:T(4,128)} %reshape.155, f32[128,4]{1,0:T(8,128)S(1)} %copy.91), kind=kLoop, calls=%fused_computation.2 | loop fusion | flops 1835008 | bytes 4720640 | tf_op jit(solution)/shard_map/reduce_sum | solution.py:193
  99.7 4.1 %all-to-all-start.3 = ((bf16[8,16,2048]{2,1,0:T(8,128)(2,1)}), bf16[8,16,2048]{2,1,0:T(8,128)(2,1)}, u32[]{:S(2)}, u32[]{:S(2)}) async-start(bf16[8,16,2048]{2,1,0:T(8,128)(2,1)} %bitcast.134), calls=%async_computation.3 | async-start | bytes 1048576 | tf_op jit(solution)/shard_map/all_to_all | solution.py:47
  103.9 2.4 %fusion.79 = f32[256,256]{1,0:T(8,128)} fusion(bf16[256,2048]{1,0:T(8,128)(2,1)S(1)} %bitcast.126, bf16[2048,256]{1,0:T(8,128)(2,1)} %param.39), kind=kOutput, calls=%fused_computation.130 | convolution fusion | flops 268435456 | bytes 2359296 | tf_op jit(solution)/shard_map/dot_general | solution.py:178
  106.2 3.9 %convolution_convert_fusion = bf16[256,2048]{1,0:T(8,128)(2,1)} fusion(bf16[256,2048]{1,0:T(8,128)(2,1)} %param.41, bf16[256,2048]{1,0:T(8,128)(2,1)S(1)} %bitcast.127, bf16[2048,256]{1,0:T(8,128)(2,1)} %param.40, f32[256,256]{1,0:T(8,128)} %fusion.79), kind=kOutput, calls=%fused_computation.3 | convolution fusion | flops 537788416 | bytes 4456448 | tf_op jit(solution)/shard_map/dot_general | solution.py:181
  110.2 4.0 %all-to-all-done.3 = bf16[8,16,2048]{2,1,0:T(8,128)(2,1)} async-done(((bf16[8,16,2048]{2,1,0:T(8,128)(2,1)}), bf16[8,16,2048]{2,1,0:T(8,128)(2,1)}, u32[]{:S(2)}, u32[]{:S(2)}) %all-to-all-start.3) | async-done | bytes 524320 | tf_op jit(solution)/shard_map/all_to_all | solution.py:47
  114.2 3.7 %all-to-all-start.4 = ((bf16[16,16,2048]{2,1,0:T(8,128)(2,1)}), bf16[16,16,2048]{2,1,0:T(8,128)(2,1)S(1)}, u32[]{:S(2)}, u32[]{:S(2)}) async-start(bf16[16,16,2048]{2,1,0:T(8,128)(2,1)} %bitcast.138), calls=%async_computation.4 | async-start | bytes 2097152 | tf_op jit(solution)/shard_map/all_to_all | solution.py:182
  117.9 1.8 %copy.101 = f32[1,128,512]{2,1,0:T(8,128)} copy(f32[1,128,512]{1,2,0:T(8,128)} %bitcast.133) | data formatting | bytes 524288 | tf_op jit(solution)/shard_map/stack;reshape | solution.py:90
  119.7 0.8 copy.100
  120.5 1.9 %pad_maximum_fusion.1 = f32[2,128,512]{2,1,0:T(8,128)} fusion(f32[1,128,512]{2,1,0:T(8,128)} %copy.101, f32[1,128,512]{2,1,0:T(8,128)} %copy.100), kind=kLoop, calls=%fused_computation.38 | loop fusion | flops 131072 | bytes 1048576 | tf_op jit(solution)/shard_map/stack | solution.py:90
  122.3 0.1 fusion.18
  122.5 1.1 convert_reduce_fusion.2
  123.6 11.8 %all-to-all-done.4 = bf16[16,16,2048]{2,1,0:T(8,128)(2,1)S(1)} async-done(((bf16[16,16,2048]{2,1,0:T(8,128)(2,1)}), bf16[16,16,2048]{2,1,0:T(8,128)(2,1)S(1)}, u32[]{:S(2)}, u32[]{:S(2)}) %all-to-all-start.4) | async-done | bytes 1048608 | tf_op jit(solution)/shard_map/all_to_all | solution.py:182
  135.5 0.1 convert_reduce_fusion
  135.6 1.6 %add_convert_fusion = bf16[16,2048]{1,0:T(8,128)(2,1)} fusion(f32[16,2048]{1,0:T(8,128)S(1)} %convert_reduce_fusion, f32[16,2048]{1,0:T(8,128)S(1)} %convert_reduce_fusion.2, f32[128,2048]{1,0:T(8,128)} %copy-done.2, s32[]{:T(128)S(6)} %select_n.41, f32[16]{0:T(128)S(1)} %fusion.18), kind=kLoop, calls=%fused_computation.63 | loop fusion | flops 131072 | bytes 458820 | tf_op jit(solution)/shard_map/convert_element_type | solution.py:196
  (50 shorter events, 0.6 us)
Async XLA Ops:
  0.6 66.9 %copy-start = (bf16[1,512,2048]{2,1,0:T(8,128)(2,1)S(1)}, bf16[1,512,2048]{2,1,0:T(8,128)(2,1)}, u32[]{:S(2)}) copy-start(bf16[1,512,2048]{2,1,0:T(8,128)(2,1)} %param.38) | copy-start | bytes 6291460
  0.6 10.7 %copy-start.10 = (s32[128,4]{0,1:T(4,128)S(1)}, s32[128,4]{0,1:T(4,128)}, u32[]{:S(2)}) copy-start(s32[128,4]{0,1:T(4,128)} %param.34) | copy-start | bytes 6148
  2.5 14.9 %all-to-all-start = ((bf16[8,128,256]{2,1,0:T(8,128)(2,1)}), bf16[8,128,256]{2,1,0:T(8,128)(2,1)S(1)}, u32[]{:S(2)}, u32[]{:S(2)}) async-start(bf16[8,128,256]{2,1,0:T(8,128)(2,1)} %broadcast_in_dim.22), calls=%async_computation | async-start | bytes 1048576 | tf_op jit(solution)/shard_map/all_to_all | solution.py:18
  10.5 2.6 %copy-start.13 = (f32[8,64]{1,0:T(8,128)S(1)}, f32[8,64]{1,0:T(8,128)}, u32[]{:S(2)}) copy-start(f32[8,64]{1,0:T(8,128)} %param.26) | copy-start | bytes 6148
  10.5 2.6 %copy-start.14 = (f32[8,64]{1,0:T(8,128)S(1)}, f32[8,64]{1,0:T(8,128)}, u32[]{:S(2)}) copy-start(f32[8,64]{1,0:T(8,128)} %param.25) | copy-start | bytes 6148
  13.3 4.6 %copy-start.11 = (f32[2048]{0:T(1024)S(1)}, f32[2048]{0:T(1024)}, u32[]{:S(2)}) copy-start(f32[2048]{0:T(1024)} %param.22) | copy-start | bytes 24580
  17.4 1.0 copy-start.7
  17.5 1.4 %copy-start.8 = (f32[2,8,64,16]{2,3,1,0:T(8,128)S(1)}, f32[2,8,64,16]{2,3,1,0:T(8,128)}, u32[]{:S(2)}) copy-start(f32[2,8,64,16]{2,3,1,0:T(8,128)} %param.28) | copy-start | bytes 196612
  17.6 1.9 %copy-start.9 = (f32[2,8,16,64]{3,2,1,0:T(8,128)S(1)}, f32[2,8,16,64]{3,2,1,0:T(8,128)}, u32[]{:S(2)}) copy-start(f32[2,8,16,64]{3,2,1,0:T(8,128)} %param.29) | copy-start | bytes 196612
  18.4 1.4 copy-start.16
  18.4 13.1 %copy-start.3 = (bf16[1024,2048]{1,0:T(8,128)(2,1)S(1)}, bf16[1024,2048]{1,0:T(8,128)(2,1)}, u32[]{:S(2)}) copy-start(bf16[1024,2048]{1,0:T(8,128)(2,1)} %param.31) | copy-start | bytes 12582916
  19.2 13.2 %copy-start.5 = (f32[128,8,64]{0,2,1:T(8,128)}, f32[128,8,64]{0,2,1:T(8,128)S(1)}, u32[]{:S(2)}) copy-start(f32[128,8,64]{0,2,1:T(8,128)S(1)} %fusion.9) | copy-start | bytes 786436
  31.5 1.9 %copy-start.12 = (f32[2048]{0:T(1024)S(1)}, f32[2048]{0:T(1024)}, u32[]{:S(2)}) copy-start(f32[2048]{0:T(1024)} %param.32) | copy-start | bytes 24580
  32.3 1.0 copy-start.2
  34.8 32.3 %copy-start.6 = (bf16[1,2048,512]{2,1,0:T(8,128)(2,1)S(1)}, bf16[1,2048,512]{2,1,0:T(8,128)(2,1)}, u32[]{:S(2)}) copy-start(bf16[1,2048,512]{2,1,0:T(8,128)(2,1)} %param.36) | copy-start | bytes 6291460
  65.9 1.2 copy-start.1
  70.9 14.4 %all-to-all-start.2 = ((bf16[16,8,2048]{2,1,0:T(8,128)(2,1)}), bf16[16,8,2048]{2,1,0:T(8,128)(2,1)S(1)}, u32[]{:S(2)}, u32[]{:S(2)}) async-start(bf16[16,8,2048]{2,1,0:T(8,128)(2,1)} %fusion), calls=%async_computation.2 | async-start | bytes 1048576 | tf_op jit(solution)/shard_map/all_to_all | solution.py:176
  93.4 10.4 %copy-start.4 = (bf16[16,16,2048]{2,1,0:T(8,128)(2,1)S(1)}, bf16[16,16,2048]{2,1,0:T(8,128)(2,1)}, u32[]{:S(2)}) copy-start(bf16[16,16,2048]{2,1,0:T(8,128)(2,1)} %slice.48) | copy-start | bytes 3145732
  99.7 14.5 %all-to-all-start.3 = ((bf16[8,16,2048]{2,1,0:T(8,128)(2,1)}), bf16[8,16,2048]{2,1,0:T(8,128)(2,1)}, u32[]{:S(2)}, u32[]{:S(2)}) async-start(bf16[8,16,2048]{2,1,0:T(8,128)(2,1)} %bitcast.134), calls=%async_computation.3 | async-start | bytes 1048576 | tf_op jit(solution)/shard_map/all_to_all | solution.py:47
  110.1 7.7 %copy-start.15 = (bf16[2048]{0:T(1024)(128)(2,1)S(1)}, bf16[2048]{0:T(1024)(128)(2,1)}, u32[]{:S(2)}) copy-start(bf16[2048]{0:T(1024)(128)(2,1)} %param.33) | copy-start | bytes 12292
  114.2 21.3 %all-to-all-start.4 = ((bf16[16,16,2048]{2,1,0:T(8,128)(2,1)}), bf16[16,16,2048]{2,1,0:T(8,128)(2,1)S(1)}, u32[]{:S(2)}, u32[]{:S(2)}) async-start(bf16[16,16,2048]{2,1,0:T(8,128)(2,1)} %bitcast.138), calls=%async_computation.4 | async-start | bytes 2097152 | tf_op jit(solution)/shard_map/all_to_all | solution.py:182
